TPU v7x, 32 devices: a whole 2x2x4 slice. The times are simulated.
32 devices in a mesh: fs: 16 (over z, y, x), tp: 2 (over core).
Axes of the slice: x: 2, y: 2, z: 4, core: 2. Of those that a mesh axis runs over, the one named last changes fastest.
Arguments:
- tokens: bfloat16 [6144, 2048], P('fs', 'tp'), may hold values from -24 to 24
- mixer_gain: float32 [2048], replicated, may hold values from 0.1 to 1.9
- pool_input: bfloat16 [2048, 1024], P('fs', 'tp'), may hold values from -0.125 to 0.125
- group_weight: bfloat16 [8, 128, 128], P('tp'), may hold values from -0.5 to 0.5
- channel_scale: float32 [1024], P('tp'), may hold values from 0.5 to 2
- pool_output: bfloat16 [1024, 2048], P('tp', 'fs'), may hold values from -0.1875 to 0.1875
- ffn_gain: float32 [2048], replicated, may hold values from 0.1 to 1.9
- gate_weight: bfloat16 [2048, 5632], P('fs', 'tp'), may hold values from -0.125 to 0.125
- up_weight: bfloat16 [2048, 5632], P('fs', 'tp'), may hold values from -0.125 to 0.125
- down_weight: bfloat16 [5632, 2048], P('tp', 'fs'), may hold values from -0.078125 to 0.078125
- final_gain: float32 [2048], P('tp'), may hold values from 0.1 to 1.9
Outputs:
- normed_out: bfloat16 [6144, 2048], P('fs', 'tp')
All inputs are finite; a program needn't handle non-finite values.
Results may differ from a plain program's by a relative error of at most 0.015.
Values may be sent and summed in bfloat16 or wider, within the bound.
No kernel may reach another device: no remote copies, remote signals or barrier semaphores. Data moves between devices by JAX's collectives and lax.ppermute only.
A program may use at most 128 MiB of HBM per device.

v0:
```python
import jax
import jax.numpy as jnp
from jax import lax
from jax.sharding import PartitionSpec as P

D = 2048
GROUP_DIM = 128
LENGTH = 128
EPS = 1e-06


def rms(values, gain):
    wide = values.astype(jnp.float32)
    scaled = wide * lax.rsqrt(jnp.mean(wide * wide, axis=-1, keepdims=True) + EPS)
    return scaled * gain


def add_rows(left, piece):
    return jnp.dot(left, piece, preferred_element_type=jnp.float32)


def local(
    tokens,
    mixer_gain,
    pool_input,
    group_weight,
    channel_scale,
    pool_output,
    ffn_gain,
    gate_weight,
    up_weight,
    down_weight,
    final_gain,
):
    full_rows = lax.all_gather(tokens, "tp", axis=1, tiled=True)
    first_normed = rms(full_rows, mixer_gain).astype(jnp.bfloat16)
    row_count = first_normed.shape[0]
    pooled_in = add_rows(first_normed, lax.all_gather(pool_input, "fs", axis=0, tiled=True)).astype(
        jnp.bfloat16
    )
    local_groups = group_weight.shape[0]
    group_ids = lax.axis_index("tp") * local_groups + jnp.arange(local_groups, dtype=jnp.int32)
    windows = jnp.left_shift(jnp.int32(2), group_ids % 4)
    later = jnp.arange(LENGTH, dtype=jnp.int32)[None, :, None]
    earlier = jnp.arange(LENGTH, dtype=jnp.int32)[None, None, :]
    reach = windows[:, None, None]
    inside = (earlier <= later) & (earlier > later - reach)
    band = inside.astype(jnp.bfloat16)
    divisor = jnp.minimum(later[:, :, 0] + 1, windows[:, None]).astype(jnp.float32)
    grid_low = pooled_in.reshape(row_count // LENGTH, LENGTH, local_groups, GROUP_DIM)
    window_sums = jnp.einsum("gts,nsgc->ntgc", band, grid_low, preferred_element_type=jnp.float32)
    average = window_sums / jnp.transpose(divisor)[None, :, :, None]
    pooled = (
        (average - grid_low.astype(jnp.float32))
        .astype(jnp.bfloat16)
        .reshape(row_count, local_groups, GROUP_DIM)
    )
    mapped = jnp.einsum("ngc,gcd->ngd", pooled, group_weight, preferred_element_type=jnp.float32)
    grouped = (mapped.reshape(row_count, local_groups * GROUP_DIM) * channel_scale).astype(
        jnp.bfloat16
    )
    mixer_terms = jnp.dot(
        grouped,
        lax.all_gather(pool_output, "fs", axis=1, tiled=True),
        preferred_element_type=jnp.float32,
    )
    mixer_out = lax.psum_scatter(
        mixer_terms.astype(jnp.bfloat16), "tp", scatter_dimension=1, tiled=True
    ).astype(jnp.float32)
    middle = (tokens.astype(jnp.float32) + mixer_out).astype(jnp.bfloat16)
    middle_rows = lax.all_gather(middle, "tp", axis=1, tiled=True)
    second_normed = rms(middle_rows, ffn_gain).astype(jnp.bfloat16)
    gate = add_rows(second_normed, lax.all_gather(gate_weight, "fs", axis=0, tiled=True))
    upward = add_rows(second_normed, lax.all_gather(up_weight, "fs", axis=0, tiled=True))
    hidden = (jax.nn.silu(gate) * upward).astype(jnp.bfloat16)
    ffn_terms = jnp.dot(
        hidden,
        lax.all_gather(down_weight, "fs", axis=1, tiled=True),
        preferred_element_type=jnp.float32,
    )
    ffn_out = lax.psum_scatter(
        ffn_terms.astype(jnp.bfloat16), "tp", scatter_dimension=1, tiled=True
    ).astype(jnp.float32)
    closing = middle.astype(jnp.float32) + ffn_out
    squares = lax.psum(jnp.sum(closing * closing, axis=1, keepdims=True), "tp")
    scaled = closing * lax.rsqrt(squares / D + EPS) * final_gain
    return scaled.astype(jnp.bfloat16)


def solution(mesh):
    placed = (
        P("fs", "tp"),
        P(),
        P("fs", "tp"),
        P("tp", None, None),
        P("tp"),
        P("tp", "fs"),
        P(),
        P("fs", "tp"),
        P("fs", "tp"),
        P("tp", "fs"),
        P("tp"),
    )
    return jax.shard_map(
        local, mesh=mesh, in_specs=placed, out_specs=P("fs", "tp"), check_vma=False
    )
```

profile of v0, /device:TPU:0, one launch (start us, length us, event | category | flops | bytes accessed | tf_op | source)
XLA Modules:
  0.0 684.9 jit_solution(15526173825975011963)
XLA Ops:
  6.5 0.7 all-gather.8.cloned.1.call-update
  7.3 0.7 all-gather.10.cloned.1.call-update
  8.1 0.7 all-gather.12.cloned.1.call-update
  9.0 12.4 %all-gather.8.cloned.1.call-done = bf16[384,2048]{1,0:T(8,128)(2,1)} async-done(((bf16[384,1024]{1,0:T(8,128)(2,1)}), bf16[384,2048]{1,0:T(8,128)(2,1)}) %all-gather.8.cloned.1.call-update) | async-done | bytes 1572880 | tf_op jit(solution)/shard_map/all_gather | solution.py:35
  21.4 1.8 fusion.1
  23.2 62.6 %all-gather.10.cloned.1.call-done = bf16[2048,512]{1,0:T(8,128)(2,1)} async-done(((bf16[128,512]{1,0:T(8,128)(2,1)}), bf16[2048,512]{1,0:T(8,128)(2,1)}) %all-gather.10.cloned.1.call-update) | async-done | bytes 2097168 | tf_op jit(solution)/shard_map/all_gather | solution.py:38
  85.8 3.1 fusion.14
  89.8 60.4 %all-gather.12.cloned.1.call-done = bf16[512,2048]{1,0:T(8,128)(2,1)} async-done(((bf16[512,128]{1,0:T(8,128)(2,1)}), bf16[512,2048]{1,0:T(8,128)(2,1)}) %all-gather.12.cloned.1.call-update) | async-done | bytes 2097168 | tf_op jit(solution)/shard_map/all_gather | solution.py:64
  150.3 3.8 convolution_convert_fusion.1
  154.1 7.2 %reduce-scatter.3.cloned.1.call-done = bf16[384,1024]{1,0:T(8,128)(2,1)} async-done(((bf16[384,2048]{1,0:T(8,128)(2,1)}), bf16[384,1024]{1,0:T(8,128)(2,1)}) %reduce-scatter.3.cloned.1.call-update) | async-done | bytes 786448 | tf_op jit(solution)/shard_map/reduce_scatter | solution.py:67
  161.4 2.3 add_convert_fusion
  164.3 0.7 all-gather.18.cloned.1.call-update
  165.1 0.7 all-gather.20.cloned.1.call-update
  166.0 8.9 %all-gather.14.cloned.1.call-done = bf16[384,2048]{1,0:T(8,128)(2,1)} async-done(((bf16[384,1024]{1,0:T(8,128)(2,1)}), bf16[384,2048]{1,0:T(8,128)(2,1)}) %all-gather.14.cloned.1.call-update) | async-done | bytes 1572880 | tf_op jit(solution)/shard_map/all_gather | solution.py:71
  174.9 1.8 fusion.4
  176.7 143.4 %all-gather.16.cloned.1.call-done = bf16[2048,2816]{1,0:T(8,128)(2,1)} async-done(((bf16[128,2816]{1,0:T(8,128)(2,1)}), bf16[2048,2816]{1,0:T(8,128)(2,1)}) %all-gather.16.cloned.1.call-update) | async-done | bytes 11534352 | tf_op jit(solution)/shard_map/all_gather | solution.py:73
  320.2 11.5 %fusion.20 = f32[384,2816]{1,0:T(8,128)} fusion(bf16[2048,2816]{1,0:T(8,128)(2,1)} %all-gather.16.cloned.1.call-done, bf16[384,2048]{1,0:T(8,128)(2,1)} %all-gather.14.cloned.1.call-done, f32[2048]{0:T(1024)S(1)} %copy-done.6, f32[384]{0:T(512)S(1)} %add_rsqrt_fusion), kind=kOutput, calls=%fused_computation.28 | convolution fusion | flops 4432330752 | bytes 17442304 | tf_op jit(solution)/shard_map/dot_general | solution.py:19
  331.7 130.8 %all-gather.18.cloned.1.call-done = bf16[2048,2816]{1,0:T(8,128)(2,1)} async-done(((bf16[128,2816]{1,0:T(8,128)(2,1)}), bf16[2048,2816]{1,0:T(8,128)(2,1)}) %all-gather.18.cloned.1.call-update) | async-done | bytes 11534352 | tf_op jit(solution)/shard_map/all_gather | solution.py:74
  462.5 183.0 %all-gather.20.cloned.1.call-done = bf16[2816,2048]{1,0:T(8,128)(2,1)} async-done(((bf16[2816,128]{1,0:T(8,128)(2,1)}), bf16[2816,2048]{1,0:T(8,128)(2,1)}) %all-gather.20.cloned.1.call-update) | async-done | bytes 11534352 | tf_op jit(solution)/shard_map/all_gather | solution.py:78
  645.5 19.3 %convolution_convert_fusion = bf16[384,2048]{1,0:T(8,128)(2,1)} fusion(bf16[2816,2048]{1,0:T(8,128)(2,1)} %all-gather.20.cloned.1.call-done, bf16[2048,2816]{1,0:T(8,128)(2,1)} %all-gather.18.cloned.1.call-done, f32[384,2816]{1,0:T(8,128)} %fusion.20, bf16[384,2048]{1,0:T(8,128)(2,1)S(1)} %copy-done.3, f32[2048]{0:T(1024)S(1)} %copy-done.6, ...), kind=kOutput, calls=%fused_computation.12 | convolution fusion | flops 8868790272 | bytes 30549504 | tf_op jit(solution)/shard_map/dot_general | solution.py:76
  664.8 7.3 %reduce-scatter.5.cloned.1.call-done = bf16[384,1024]{1,0:T(8,128)(2,1)} async-done(((bf16[384,2048]{1,0:T(8,128)(2,1)}), bf16[384,1024]{1,0:T(8,128)(2,1)}) %reduce-scatter.5.cloned.1.call-update) | async-done | bytes 786448 | tf_op jit(solution)/shard_map/reduce_scatter | solution.py:81
  672.1 1.5 multiply_reduce_fusion
  673.6 2.5 psum.7
  676.1 2.3 multiply_convert_fusion
  (40 shorter events, 2.2 us)
Async XLA Ops:
  6.5 82.8 %copy-start = (bf16[4,128,128]{2,1,0:T(8,128)(2,1)S(1)}, bf16[4,128,128]{2,1,0:T(8,128)(2,1)}, u32[]{:S(2)}) copy-start(bf16[4,128,128]{2,1,0:T(8,128)(2,1)} %param.14) | copy-start | bytes 393220
  6.5 14.9 %all-gather.8.cloned.1.call-start = ((), (), s32[]{:S(2)}) async-start(), calls=%async_computation.2 | async-start | bytes 2359296 | tf_op jit(solution)/shard_map/all_gather | solution.py:35
  7.3 78.5 %all-gather.10.cloned.1.call-start = ((), (), s32[]{:S(2)}) async-start(), calls=%async_computation.3 | async-start | bytes 2228224 | tf_op jit(solution)/shard_map/all_gather | solution.py:38
  8.0 142.3 %all-gather.12.cloned.1.call-start = ((), (), s32[]{:S(2)}) async-start(), calls=%async_computation.4 | async-start | bytes 2228224 | tf_op jit(solution)/shard_map/all_gather | solution.py:64
  8.7 152.6 %reduce-scatter.3.cloned.1.call-start = ((), (), s32[]{:S(2)}) async-start(), calls=%async_computation.5 | async-start | bytes 2359296 | tf_op jit(solution)/shard_map/reduce_scatter | solution.py:67
  88.9 0.8 copy-start.5
  89.7 71.7 %copy-start.2 = (bf16[384,1024]{1,0:T(8,128)(2,1)S(1)}, bf16[384,1024]{1,0:T(8,128)(2,1)}, u32[]{:S(2)}) copy-start(bf16[384,1024]{1,0:T(8,128)(2,1)} %param.11) | copy-start | bytes 2359300
  154.1 166.1 %copy-start.6 = (f32[2048]{0:T(1024)S(1)}, f32[2048]{0:T(1024)}, u32[]{:S(2)}) copy-start(f32[2048]{0:T(1024)} %param.17) | copy-start | bytes 24580
  154.1 20.8 %all-gather.14.cloned.1.call-start = ((), (), s32[]{:S(2)}) async-start(), calls=%async_computation.6 | async-start | bytes 2359296 | tf_op jit(solution)/shard_map/all_gather | solution.py:71
  163.7 156.5 %all-gather.16.cloned.1.call-start = ((), (), s32[]{:S(2)}) async-start(), calls=%async_computation.7 | async-start | bytes 12255232 | tf_op jit(solution)/shard_map/all_gather | solution.py:73
  164.3 298.3 %all-gather.18.cloned.1.call-start = ((), (), s32[]{:S(2)}) async-start(), calls=%async_computation.8 | async-start | bytes 12255232 | tf_op jit(solution)/shard_map/all_gather | solution.py:74
  165.0 480.5 %all-gather.20.cloned.1.call-start = ((), (), s32[]{:S(2)}) async-start(), calls=%async_computation.9 | async-start | bytes 12255232 | tf_op jit(solution)/shard_map/all_gather | solution.py:78
  165.8 506.3 %reduce-scatter.5.cloned.1.call-start = ((), (), s32[]{:S(2)}) async-start(), calls=%async_computation.10 | async-start | bytes 2359296 | tf_op jit(solution)/shard_map/reduce_scatter | solution.py:81
  176.7 468.8 %copy-start.3 = (bf16[384,2048]{1,0:T(8,128)(2,1)S(1)}, bf16[384,2048]{1,0:T(8,128)(2,1)}, u32[]{:S(2)}) copy-start(bf16[384,2048]{1,0:T(8,128)(2,1)} %all-gather.14.cloned.1.call-done) | copy-start | bytes 4718596
  331.7 340.4 %copy-start.1 = (bf16[384,1024]{1,0:T(8,128)(2,1)S(1)}, bf16[384,1024]{1,0:T(8,128)(2,1)}, u32[]{:S(2)}) copy-start(bf16[384,1024]{1,0:T(8,128)(2,1)} %add_convert_fusion) | copy-start | bytes 2359300
  664.8 11.3 %copy-start.4 = (f32[1024]{0:T(1024)S(1)}, f32[1024]{0:T(1024)}, u32[]{:S(2)}) copy-start(f32[1024]{0:T(1024)} %param.21) | copy-start | bytes 12292
Sparse Core Ops, SparseCore 0:
  8.9 12.5 all-gather.7
  24.2 61.5 all-gather.9
  88.5 61.7 all-gather.11
  154.2 7.1 reduce-scatter.2
  163.8 11.0 all-gather.13
  177.5 142.5 all-gather.15
  322.9 139.5 all-gather.17
  465.3 180.2 all-gather.19
  664.9 7.1 reduce-scatter.4
where the time goes:
time: 685 us
  waiting for transfers between devices  620 us (91%)
  matrix products  38.3 us (6%)
  between operations  13.3 us (2%)
  other arithmetic  10 us (1%)
    all_gather x1, waiting for transfers between devices, local(): lax.all_gather(down_weight, 'fs', axis=1, tiled=True)  183 us
    all_gather x1, waiting for transfers between devices, local(): lax.all_gather(gate_weight, 'fs', axis=0, tiled=True)  143 us
    all_gather x1, waiting for transfers between devices, local(): lax.all_gather(up_weight, 'fs', axis=0, tiled=True)  131 us
    all_gather x1, waiting for transfers between devices, local(): lax.all_gather(pool_input, 'fs', axis=0, tiled=True)  62.6 us
    all_gather x1, waiting for transfers between devices, local(): lax.all_gather(pool_output, 'fs', axis=1, tiled=True)  60.4 us
    dot_general x1, matrix products, local(): jnp.dot(hidden, lax.all_gather(down_weight, 'fs', axis=1, tiled=True), pr...  19.3 us
    dot_general x2, matrix products, add_rows(): return jnp.dot(left, piece, preferred_element_type=jnp.float32)  14.6 us
  transfers between devices with their start and end apart: 9, of which 9 were waited for; matrix products, arithmetic and copies ran while one was open for 3% of the time, Pallas kernels for 0%

commit v1 on v0

--- a/solution.py
+++ b/solution.py
@@ -7,6 +7,9 @@
 GROUP_DIM = 128
 LENGTH = 128
 EPS = 1e-06
+_connect_threads = lambda inputs, axis_name: jnp.concatenate(
+    lax.all_to_all(jnp.stack(lax.axis_size(axis_name) * [inputs]), axis_name, 0, 0), axis=1
+)
 
 
 def rms(values, gain):
@@ -74,9 +77,7 @@
     upward = add_rows(second_normed, lax.all_gather(up_weight, "fs", axis=0, tiled=True))
     hidden = (jax.nn.silu(gate) * upward).astype(jnp.bfloat16)
     ffn_terms = jnp.dot(
-        hidden,
-        lax.all_gather(down_weight, "fs", axis=1, tiled=True),
-        preferred_element_type=jnp.float32,
+        hidden, _connect_threads(down_weight, "fs"), preferred_element_type=jnp.float32
     )
     ffn_out = lax.psum_scatter(
         ffn_terms.astype(jnp.bfloat16), "tp", scatter_dimension=1, tiled=True

time: 685 us -> 723 us (1.055)
  waiting for transfers between devices: 620 us -> 643 us
    all_gather x1, waiting for transfers between devices: 143 us -> 348 us  [local(): lax.all_gather(gate_weight, 'fs', axis=0, tiled=True)]
    all_gather x1 -> x0, waiting for transfers between devices: 183 us -> none  [local(): lax.all_gather(down_weight, 'fs', axis=1, tiled=True)]
    all_gather x1, waiting for transfers between devices: 131 us -> 142 us  [local(): lax.all_gather(up_weight, 'fs', axis=0, tiled=True)]
    all_gather x1, waiting for transfers between devices: 8.92 us -> 0.02 us  [local(): middle_rows = lax.all_gather(middle, 'tp', axis=1, tiled=True)]
  transfers between devices with their start and end apart: 9 -> 9, of which waited for: 9 -> 7; matrix products, arithmetic and copies ran while one was open for 3% -> 3% of each run, Pallas kernels for 0% -> 0%
where the time goes in v1:
time: 723 us; the launch traced here: 722 us
  waiting for transfers between devices  643 us (89%)
  matrix products  40.5 us (6%)
  between operations  13.6 us (2%)
  other arithmetic  10 us (1%)
  starting transfers between devices  7.53 us (1%)
    all_gather x1, waiting for transfers between devices, local(): lax.all_gather(gate_weight, 'fs', axis=0, tiled=True)  348 us
    all_gather x1, waiting for transfers between devices, local(): lax.all_gather(up_weight, 'fs', axis=0, tiled=True)  142 us
    all_gather x1, waiting for transfers between devices, local(): lax.all_gather(pool_input, 'fs', axis=0, tiled=True)  62.6 us
    all_gather x1, waiting for transfers between devices, local(): lax.all_gather(pool_output, 'fs', axis=1, tiled=True)  60.4 us
    dot_general x1, matrix products, local(): jnp.dot(hidden, _connect_threads(down_weight, 'fs'), preferred_element_ty...  21.5 us
    dot_general x2, matrix products, add_rows(): return jnp.dot(left, piece, preferred_element_type=jnp.float32)  14.5 us
  transfers between devices with their start and end apart: 9, of which 7 were waited for; matrix products, arithmetic and copies ran while one was open for 3% of the time, Pallas kernels for 0%

profile of v1, /device:TPU:0, one launch (start us, length us, event | category | flops | bytes accessed | tf_op | source)
XLA Modules:
  0.0 722.5 jit_solution(14741517472112223155)
XLA Ops:
  6.5 0.7 all-gather.7.cloned.1.call-update
  7.3 0.7 all-gather.9.cloned.1.call-update
  8.1 0.7 all-gather.11.cloned.1.call-update
  9.0 12.4 %all-gather.7.cloned.1.call-done = bf16[384,2048]{1,0:T(8,128)(2,1)} async-done(((bf16[384,1024]{1,0:T(8,128)(2,1)}), bf16[384,2048]{1,0:T(8,128)(2,1)}) %all-gather.7.cloned.1.call-update) | async-done | bytes 1572880 | tf_op jit(solution)/shard_map/all_gather | solution.py:38
  21.4 1.8 fusion.1
  23.2 62.6 %all-gather.9.cloned.1.call-done = bf16[2048,512]{1,0:T(8,128)(2,1)} async-done(((bf16[128,512]{1,0:T(8,128)(2,1)}), bf16[2048,512]{1,0:T(8,128)(2,1)}) %all-gather.9.cloned.1.call-update) | async-done | bytes 2097168 | tf_op jit(solution)/shard_map/all_gather | solution.py:41
  85.8 3.1 fusion.14
  89.8 60.4 %all-gather.11.cloned.1.call-done = bf16[512,2048]{1,0:T(8,128)(2,1)} async-done(((bf16[512,128]{1,0:T(8,128)(2,1)}), bf16[512,2048]{1,0:T(8,128)(2,1)}) %all-gather.11.cloned.1.call-update) | async-done | bytes 2097168 | tf_op jit(solution)/shard_map/all_gather | solution.py:67
  150.3 3.8 convolution_convert_fusion.1
  154.1 7.2 %reduce-scatter.3.cloned.1.call-done = bf16[384,1024]{1,0:T(8,128)(2,1)} async-done(((bf16[384,2048]{1,0:T(8,128)(2,1)}), bf16[384,1024]{1,0:T(8,128)(2,1)}) %reduce-scatter.3.cloned.1.call-update) | async-done | bytes 786448 | tf_op jit(solution)/shard_map/reduce_scatter | solution.py:70
  161.3 2.3 add_convert_fusion
  163.7 0.5 all-gather.15.cloned.1.call-update
  164.6 5.3 stack.2
  169.9 7.1 all-to-all-start
  177.0 0.7 all-gather.17.cloned.1.call-update
  177.9 1.8 fusion.4
  179.7 347.8 %all-gather.15.cloned.1.call-done = bf16[2048,2816]{1,0:T(8,128)(2,1)} async-done(((bf16[128,2816]{1,0:T(8,128)(2,1)}), bf16[2048,2816]{1,0:T(8,128)(2,1)}) %all-gather.15.cloned.1.call-update) | async-done | bytes 11534352 | tf_op jit(solution)/shard_map/all_gather | solution.py:76
  527.5 11.4 %fusion.20 = f32[384,2816]{1,0:T(8,128)} fusion(bf16[2048,2816]{1,0:T(8,128)(2,1)} %all-gather.15.cloned.1.call-done, bf16[384,2048]{1,0:T(8,128)(2,1)} %all-gather.13.cloned.1.call-done, f32[2048]{0:T(1024)S(1)} %copy-done.8, f32[384]{0:T(512)S(1)} %add_rsqrt_fusion), kind=kOutput, calls=%fused_computation.28 | convolution fusion | flops 4432330752 | bytes 17442304 | tf_op jit(solution)/shard_map/dot_general | solution.py:22
  539.0 141.5 %all-gather.17.cloned.1.call-done = bf16[2048,2816]{1,0:T(8,128)(2,1)} async-done(((bf16[128,2816]{1,0:T(8,128)(2,1)}), bf16[2048,2816]{1,0:T(8,128)(2,1)}) %all-gather.17.cloned.1.call-update) | async-done | bytes 11534352 | tf_op jit(solution)/shard_map/all_gather | solution.py:77
  680.5 21.5 %convolution_convert_fusion = bf16[384,2048]{1,0:T(8,128)(2,1)} fusion(bf16[2816,2048]{0,1:T(8,128)(2,1)} %bitcast.7, bf16[2048,2816]{1,0:T(8,128)(2,1)} %all-gather.17.cloned.1.call-done, f32[384,2816]{1,0:T(8,128)} %fusion.20, bf16[384,2048]{1,0:T(8,128)(2,1)S(1)} %copy-done.4, f32[2048]{0:T(1024)S(1)} %copy-done.8, f32[384]{0:T(512)S(1)} %add_rsqrt_fusion), kind=kOutput, calls=%fused_computation.12 | convolution fusion | flops 8868790272 | bytes 30549504 | tf_op jit(solution)/shard_map/dot_general | solution.py:79
  702.0 7.3 %reduce-scatter.5.cloned.1.call-done = bf16[384,1024]{1,0:T(8,128)(2,1)} async-done(((bf16[384,2048]{1,0:T(8,128)(2,1)}), bf16[384,1024]{1,0:T(8,128)(2,1)}) %reduce-scatter.5.cloned.1.call-update) | async-done | bytes 786448 | tf_op jit(solution)/shard_map/reduce_scatter | solution.py:82
  709.3 1.5 multiply_reduce_fusion
  710.8 2.5 psum.7
  713.3 2.3 multiply_convert_fusion
  (45 shorter events, 1.9 us)
Async XLA Ops:
  6.5 82.8 %copy-start = (bf16[4,128,128]{2,1,0:T(8,128)(2,1)S(1)}, bf16[4,128,128]{2,1,0:T(8,128)(2,1)}, u32[]{:S(2)}) copy-start(bf16[4,128,128]{2,1,0:T(8,128)(2,1)} %param.14) | copy-start | bytes 393220
  6.5 14.9 %all-gather.7.cloned.1.call-start = ((), (), s32[]{:S(2)}) async-start(), calls=%async_computation.3 | async-start | bytes 2359296 | tf_op jit(solution)/shard_map/all_gather | solution.py:38
  7.3 78.5 %all-gather.9.cloned.1.call-start = ((), (), s32[]{:S(2)}) async-start(), calls=%async_computation.4 | async-start | bytes 2228224 | tf_op jit(solution)/shard_map/all_gather | solution.py:41
  8.0 142.3 %all-gather.11.cloned.1.call-start = ((), (), s32[]{:S(2)}) async-start(), calls=%async_computation.5 | async-start | bytes 2228224 | tf_op jit(solution)/shard_map/all_gather | solution.py:67
  8.7 152.6 %reduce-scatter.3.cloned.1.call-start = ((), (), s32[]{:S(2)}) async-start(), calls=%async_computation.6 | async-start | bytes 2359296 | tf_op jit(solution)/shard_map/reduce_scatter | solution.py:70
  88.9 0.8 copy-start.7
  89.7 71.7 %copy-start.3 = (bf16[384,1024]{1,0:T(8,128)(2,1)S(1)}, bf16[384,1024]{1,0:T(8,128)(2,1)}, u32[]{:S(2)}) copy-start(bf16[384,1024]{1,0:T(8,128)(2,1)} %param.11) | copy-start | bytes 2359300
  154.0 10.2 %copy-start.5 = (bf16[2816,128]{1,0:T(8,128)(2,1)S(1)}, bf16[2816,128]{1,0:T(8,128)(2,1)}, u32[]{:S(2)}) copy-start(bf16[2816,128]{1,0:T(8,128)(2,1)} %param.20) | copy-start | bytes 2162692
  154.1 23.9 %all-gather.13.cloned.1.call-start = ((), (), s32[]{:S(2)}) async-start(), calls=%async_computation.7 | async-start | bytes 2359296 | tf_op jit(solution)/shard_map/all_gather | solution.py:74
  163.7 363.8 %all-gather.15.cloned.1.call-start = ((), (), s32[]{:S(2)}) async-start(), calls=%async_computation.8 | async-start | bytes 12255232 | tf_op jit(solution)/shard_map/all_gather | solution.py:76
  169.9 357.7 %copy-start.8 = (f32[2048]{0:T(1024)S(1)}, f32[2048]{0:T(1024)}, u32[]{:S(2)}) copy-start(f32[2048]{0:T(1024)} %param.17) | copy-start | bytes 24580
  169.9 369.1 %all-to-all-start = ((bf16[16,2816,128]{1,2,0:T(8,128)(2,1)}), bf16[16,2816,128]{1,2,0:T(8,128)(2,1)}, u32[]{:S(2)}, u32[]{:S(2)}) async-start(bf16[16,2816,128]{1,2,0:T(8,128)(2,1)} %stack.2), calls=%async_computation.1 | async-start | bytes 23068672 | tf_op jit(solution)/shard_map/all_to_all | solution.py:11
  176.9 503.6 %all-gather.17.cloned.1.call-start = ((), (), s32[]{:S(2)}) async-start(), calls=%async_computation.9 | async-start | bytes 12255232 | tf_op jit(solution)/shard_map/all_gather | solution.py:77
  177.7 531.6 %reduce-scatter.5.cloned.1.call-start = ((), (), s32[]{:S(2)}) async-start(), calls=%async_computation.10 | async-start | bytes 2359296 | tf_op jit(solution)/shard_map/reduce_scatter | solution.py:82
  179.7 500.8 %copy-start.4 = (bf16[384,2048]{1,0:T(8,128)(2,1)S(1)}, bf16[384,2048]{1,0:T(8,128)(2,1)}, u32[]{:S(2)}) copy-start(bf16[384,2048]{1,0:T(8,128)(2,1)} %all-gather.13.cloned.1.call-done) | copy-start | bytes 4718596
  680.5 28.8 %copy-start.2 = (bf16[384,1024]{1,0:T(8,128)(2,1)S(1)}, bf16[384,1024]{1,0:T(8,128)(2,1)}, u32[]{:S(2)}) copy-start(bf16[384,1024]{1,0:T(8,128)(2,1)} %add_convert_fusion) | copy-start | bytes 2359300
  680.5 35.1 %copy-start.1 = (bf16[4,128,128]{2,1,0:T(8,128)(2,1)S(1)}, bf16[4,128,128]{2,1,0:T(8,128)(2,1)}, u32[]{:S(2)}) copy-start(bf16[4,128,128]{2,1,0:T(8,128)(2,1)} %param.14) | copy-start | bytes 393220
  702.0 11.3 %copy-start.6 = (f32[1024]{0:T(1024)S(1)}, f32[1024]{0:T(1024)}, u32[]{:S(2)}) copy-start(f32[1024]{0:T(1024)} %param.21) | copy-start | bytes 12292
Sparse Core Ops, SparseCore 0:
  8.9 12.5 all-gather.6
  24.2 61.5 all-gather.8
  88.5 61.7 all-gather.10
  154.2 7.1 reduce-scatter.2
  163.8 11.0 all-gather.12
  177.5 349.9 all-gather.14
  530.3 150.1 all-gather.16
  702.2 7.1 reduce-scatter.4
